TPU v7x, 32 devices: a whole 2x2x4 slice. The times are simulated.
32 devices in a mesh: ep: 16 (over z, y, x), tp: 2 (over core).
Axes of the slice: x: 2, y: 2, z: 4, core: 2. Of those that a mesh axis runs over, the one named last changes fastest.
Arguments:
- hidden: bfloat16 [256, 2048], P('ep'), may hold values from -6 to 6
- attn_gain: bfloat16 [2048], replicated, may hold values from 0.099609375 to 1.8984375
- query_weight: bfloat16 [2048, 2048], P(None, 'tp'), may hold values from -0.125 to 0.125
- key_weight: bfloat16 [2048, 128], P(None, 'tp'), may hold values from -0.125 to 0.125
- value_weight: bfloat16 [2048, 128], P(None, 'tp'), may hold values from -0.125 to 0.125
- forget_weight: bfloat16 [2048, 32], P(None, 'tp'), may hold values from -0.125 to 0.125
- forget_bias: float32 [32], P('tp'), may hold values from -1 to 4
- cache_keys: bfloat16 [256, 2, 64, 1024], P('ep', 'tp'), may hold values from -64 to 64
- cache_values: bfloat16 [256, 2, 64, 1024], P('ep', 'tp'), may hold values from -6 to 6
- cache_logsum: float32 [256, 32, 1024], P('ep', 'tp'), may hold values from -144 to 0, as said below
- lengths: int32 [256], P('ep'), may hold values from 2 to 1023, as said below
- out_weight: bfloat16 [2048, 2048], P('ep'), may hold values from -0.125 to 0.125
- ffn_gain: bfloat16 [2048], replicated, may hold values from 0.099609375 to 1.8984375
- expert_ids: int32 [256, 6], P('ep'), may hold values from 0 to 15, all different within a row; in each aligned block of 16 rows (0 to 15, 16 to 31, ...) at most 12 rows name the same one
- expert_scores: float32 [256, 6], P('ep'), may hold values from 0.1 to 1
- gate_weights: bfloat16 [16, 2048, 512], P('ep', None, 'tp'), may hold values from -0.125 to 0.125
- up_weights: bfloat16 [16, 2048, 512], P('ep', None, 'tp'), may hold values from -0.125 to 0.125
- down_weights: bfloat16 [16, 512, 2048], P('ep', 'tp'), may hold values from -0.25 to 0.25
Outputs:
- updated: bfloat16 [256, 2048], P('ep')
- new_key: bfloat16 [256, 2, 64], P('ep', 'tp')
- new_value: bfloat16 [256, 2, 64], P('ep', 'tp')
- new_logsum: float32 [256, 32], P('ep', 'tp')
Inputs may be any that keep to these rules, and one draw needn't show every extreme that they name: `cache_logsum`: non-increasing along the positions. The new token stands at position lengths; some sequence has 1023 cached positions. `expert_ids`: each row names 6 different experts; the rows of one index of ep name one expert at most 12 times.
All inputs are finite; a program needn't handle non-finite values.
Results may differ from a plain program's by a relative error of at most 0.006.
Values may be sent and summed in bfloat16 or wider, within the bound.
A program may use at most 64 MiB of HBM per device.

v0:
```python
import jax
import jax.numpy as jnp
from jax import lax
from jax.sharding import PartitionSpec as P

HD = 64
TOP_K = 6


epsilon = 1e-06


def root_norm(values_in, gain):
    floats = values_in.astype(jnp.float32)
    inv_root = lax.rsqrt(jnp.mean(floats * floats, axis=-1, keepdims=True) + epsilon)
    return floats * inv_root * gain.astype(jnp.float32)


def per_device(
    hidden,
    attn_gain,
    query_weight,
    key_weight,
    value_weight,
    forget_weight,
    forget_bias,
    cache_keys,
    cache_values,
    cache_logsum,
    lengths,
    out_weight,
    ffn_gain,
    expert_ids,
    expert_scores,
    gate_weights,
    up_weights,
    down_weights,
):
    rows_here = hidden.shape[0]
    query_heads = query_weight.shape[1] // HD
    key_heads = key_weight.shape[1] // HD
    group_size = query_heads // key_heads
    cache_len = cache_keys.shape[-1]
    score_scale = HD ** (-0.5)
    normed = root_norm(hidden, attn_gain).astype(jnp.bfloat16)
    queries = jnp.dot(normed, query_weight, preferred_element_type=jnp.float32).astype(jnp.bfloat16)
    key_new = (
        jnp.dot(normed, key_weight, preferred_element_type=jnp.float32)
        .astype(jnp.bfloat16)
        .reshape(rows_here, key_heads, HD)
    )
    value_new = (
        jnp.dot(normed, value_weight, preferred_element_type=jnp.float32)
        .astype(jnp.bfloat16)
        .reshape(rows_here, key_heads, HD)
    )
    log_forget = jax.nn.log_sigmoid(
        jnp.dot(normed, forget_weight, preferred_element_type=jnp.float32) + forget_bias
    )
    positions = jnp.arange(cache_len, dtype=jnp.int32)
    is_last = positions[None, :] == (lengths - 1)[:, None]
    new_logsum = jnp.sum(jnp.where(is_last[:, None, :], cache_logsum, 0.0), axis=-1) + log_forget
    grouped = queries.reshape(rows_here, key_heads, group_size, HD)
    scores = jnp.einsum("sgjd,sgdp->sgjp", grouped, cache_keys, preferred_element_type=jnp.float32)
    scores = scores.reshape(rows_here, query_heads, cache_len) * score_scale
    scores = scores + new_logsum[:, :, None] - cache_logsum
    is_live = positions[None, :] < lengths[:, None]
    scores = jnp.where(is_live[:, None, :], scores, -jnp.inf)
    own_score = (
        jnp.einsum("sgjd,sgd->sgj", grouped, key_new, preferred_element_type=jnp.float32).reshape(
            rows_here, query_heads
        )
        * score_scale
    )
    top_score = jnp.maximum(jnp.max(scores, axis=-1), own_score)
    past_exp = jnp.exp(scores - top_score[:, :, None])
    own_exp = jnp.exp(own_score - top_score)
    denominator = jnp.sum(past_exp, axis=-1) + own_exp
    past_weight = (past_exp / denominator[:, :, None]).astype(jnp.bfloat16)
    own_weight = (own_exp / denominator).astype(jnp.bfloat16)
    attended = jnp.einsum(
        "sgjp,sgdp->sgjd",
        past_weight.reshape(rows_here, key_heads, group_size, cache_len),
        cache_values,
        preferred_element_type=jnp.float32,
    )
    attended = (
        attended
        + own_weight.astype(jnp.float32).reshape(rows_here, key_heads, group_size)[:, :, :, None]
        * value_new.astype(jnp.float32)[:, :, None, :]
    )
    attended = attended.reshape(rows_here, query_heads * HD).astype(jnp.bfloat16)
    whole_heads = lax.all_gather(attended, "tp", axis=1, tiled=True)
    projected = lax.dot_general(
        lax.all_gather(whole_heads, "ep", axis=0, tiled=True),
        out_weight,
        (((1,), (1,)), ((), ())),
        preferred_element_type=jnp.float32,
    ).astype(jnp.bfloat16)
    mixed = lax.all_to_all(projected, "ep", split_axis=0, concat_axis=1, tiled=True)
    residual = hidden.astype(jnp.float32) + mixed.astype(jnp.float32)
    ffn_in = root_norm(residual, ffn_gain).astype(jnp.bfloat16)
    ep_size = lax.axis_size("ep")
    local_experts = gate_weights.shape[0]
    experts = ep_size * local_experts
    route_count = rows_here * TOP_K
    capacity = 2 * ((route_count + experts - 1) // experts)
    flat_ids = expert_ids.reshape(route_count)
    onehot = (flat_ids[:, None] == jnp.arange(experts, dtype=jnp.int32)[None, :]).astype(jnp.int32)
    running = jnp.cumsum(onehot, axis=0)
    slot_index = jnp.sum(running * onehot, axis=1) - 1
    target = flat_ids * capacity + slot_index
    dispatch_map = (
        target[:, None] == jnp.arange(experts * capacity, dtype=jnp.int32)[None, :]
    ).astype(jnp.bfloat16)
    route_rows = jnp.repeat(ffn_in, TOP_K, axis=0)
    outgoing = lax.dot_general(
        dispatch_map, route_rows, (((0,), (0,)), ((), ())), preferred_element_type=jnp.float32
    )
    outgoing = outgoing.astype(jnp.bfloat16).reshape(
        ep_size, local_experts, capacity, ffn_in.shape[1]
    )
    arrived = lax.all_to_all(outgoing, "ep", split_axis=0, concat_axis=0, tiled=True)
    gate_act = jnp.einsum(
        "sekd,edf->sekf", arrived, gate_weights, preferred_element_type=jnp.float32
    )
    up_act = jnp.einsum("sekd,edf->sekf", arrived, up_weights, preferred_element_type=jnp.float32)
    hidden_act = (jax.nn.silu(gate_act) * up_act).astype(jnp.bfloat16)
    partial_out = jnp.einsum(
        "sekf,efd->sekd", hidden_act, down_weights, preferred_element_type=jnp.float32
    )
    half_sum = lax.psum_scatter(
        partial_out.astype(jnp.bfloat16), "tp", scatter_dimension=3, tiled=True
    )
    sent_back = lax.all_to_all(half_sum, "ep", split_axis=0, concat_axis=0, tiled=True)
    share_width = sent_back.shape[-1]
    picked = jnp.dot(
        dispatch_map,
        sent_back.reshape(experts * capacity, share_width),
        preferred_element_type=jnp.float32,
    )
    route_weight = expert_scores / jnp.sum(expert_scores, axis=-1, keepdims=True)
    expert_mix = jnp.sum(
        picked.reshape(rows_here, TOP_K, share_width) * route_weight[:, :, None], axis=1
    )
    own_part = lax.dynamic_slice_in_dim(
        residual, lax.axis_index("tp") * share_width, share_width, 1
    )
    updated = lax.all_gather((own_part + expert_mix).astype(jnp.bfloat16), "tp", axis=1, tiled=True)
    return (updated, key_new, value_new, new_logsum)


def solution(mesh):
    in_specs = (
        P("ep", None),
        P(),
        P(None, "tp"),
        P(None, "tp"),
        P(None, "tp"),
        P(None, "tp"),
        P("tp"),
        P("ep", "tp", None, None),
        P("ep", "tp", None, None),
        P("ep", "tp", None),
        P("ep"),
        P("ep", None),
        P(),
        P("ep", None),
        P("ep", None),
        P("ep", None, "tp"),
        P("ep", None, "tp"),
        P("ep", "tp", None),
    )
    out_specs = (P("ep", None), P("ep", "tp", None), P("ep", "tp", None), P("ep", "tp"))
    return jax.shard_map(
        per_device, mesh=mesh, in_specs=in_specs, out_specs=out_specs, check_vma=False
    )
```

profile of v0, /device:TPU:1, one launch (start us, length us, event | category | flops | bytes accessed | tf_op | source)
XLA Modules:
  0.0 167.3 jit_solution(6196648160617285266)
XLA Ops:
  7.2 0.8 broadcast_add_fusion.1
  8.0 0.7 iota_compare_fusion.4
  8.8 0.7 convert_element_type.86
  9.5 1.0 fusion.48
  10.5 3.0 %convolution_convert_fusion.3 = bf16[16,1024]{1,0:T(8,128)(2,1)S(1)} fusion(bf16[2048,1024]{1,0:T(8,128)(2,1)} %param.20, bf16[16,2048]{1,0:T(8,128)(2,1)} %param.18, f32[2048]{0:T(1024)S(1)} %convert_element_type.86, f32[16]{0:T(128)S(1)} %add_rsqrt_fusion.1), kind=kOutput, calls=%fused_computation.21 | convolution fusion | flops 67256320 | bytes 4300864 | tf_op jit(solution)/shard_map/dot_general | solution.py:46
  13.7 1.2 convolution_convert_fusion.5
  14.9 0.2 select_reduce_fusion
  15.2 0.2 fusion.58
  15.5 0.5 fusion.68
  16.1 0.3 fusion.31
  16.5 0.8 fusion.69
  17.3 0.7 fusion.23
  18.2 2.0 %all_gather.9 = bf16[16,2048]{1,0:T(8,128)(2,1)} all-gather(bf16[16,1024]{1,0:T(8,128)(2,1)S(1)} %convert_element_type.96), channel_id=1, replica_groups=mesh['ep'=16,'tp'=2] {'tp'}, dimensions={1}, use_global_device_ids=true | all-gather | bytes 98304 | tf_op jit(solution)/shard_map/all_gather | solution.py:93
  20.6 0.2 select_reduce_fusion.1
  20.8 54.7 %all-gather.2.cloned.1.call-done = bf16[256,2048]{1,0:T(8,128)(2,1)} async-done(((bf16[16,2048]{1,0:T(8,128)(2,1)}), bf16[256,2048]{1,0:T(8,128)(2,1)}) %all-gather.2.cloned.1.call-update) | async-done | bytes 1048592 | tf_op jit(solution)/shard_map/all_gather | solution.py:95
  75.5 2.3 %convolution_convert_fusion.2 = bf16[256,128]{1,0:T(8,128)(2,1)} fusion(bf16[256,2048]{1,0:T(8,128)(2,1)} %all-gather.2.cloned.1.call-done, bf16[128,2048]{1,0:T(8,128)(2,1)S(1)} %copy-done.4), kind=kOutput, calls=%fused_computation.20 | convolution fusion | flops 134250496 | bytes 1638400 | tf_op jit(solution)/shard_map/dot_general | solution.py:94
  77.8 4.0 %all-to-all-start = ((bf16[16,16,128]{2,1,0:T(8,128)(2,1)}), bf16[16,16,128]{2,1,0:T(8,128)(2,1)S(1)}, u32[]{:S(2)}, u32[]{:S(2)}) async-start(bf16[16,16,128]{2,1,0:T(8,128)(2,1)} %bitcast.5), calls=%async_computation | async-start | bytes 131072 | tf_op jit(solution)/shard_map/all_to_all | solution.py:100
  81.9 6.3 %all-to-all-done = bf16[16,16,128]{2,1,0:T(8,128)(2,1)S(1)} async-done(((bf16[16,16,128]{2,1,0:T(8,128)(2,1)}), bf16[16,16,128]{2,1,0:T(8,128)(2,1)S(1)}, u32[]{:S(2)}, u32[]{:S(2)}) %all-to-all-start) | async-done | bytes 65568 | tf_op jit(solution)/shard_map/all_to_all | solution.py:100
  88.7 1.4 convolution_convert_fusion.1
  90.0 1.3 reshape.207
  91.3 26.2 %all_to_all.23 = bf16[16,1,12,2048]{3,2,1,0:T(8,128)(2,1)S(1)} all-to-all(bf16[16,1,12,2048]{3,2,1,0:T(8,128)(2,1)S(1)} %bitcast.98), channel_id=1, replica_groups=mesh['ep'=16,'tp'=2] {'ep'}, dimensions={0} | all-to-all | bytes 1572864 | tf_op jit(solution)/shard_map/all_to_all | solution.py:123
  117.5 1.0 copy-done.3
  118.5 0.6 convolution_bitcast_fusion.1
  119.1 0.6 copy-done.12
  119.7 3.5 %fusion = bf16[16,1,12,2048]{3,0,2,1:T(8,128)(2,1)} fusion(bf16[1,256,2048]{2,1,0:T(8,128)(2,1)S(1)} %copy-done.12, bf16[1,2048,256]{2,1,0:T(8,128)(2,1)} %param.34, bf16[16,1,12,2048]{3,2,1,0:T(8,128)(2,1)} %copy-done.3, f32[16,1,12,256]{3,0,2,1:T(8,128)S(1)} %convolution_bitcast_fusion.1), kind=kOutput, calls=%fused_computation.2 | convolution fusion | flops 403341312 | bytes 3866624 | tf_op jit(solution)/shard_map/sekf,efd->sekd/dot_general | solution.py:129
  123.3 10.1 %reduce-scatter.2.cloned.1.call-done = bf16[16,1,12,1024]{3,0,2,1:T(8,128)(2,1)} async-done(((bf16[16,1,12,2048]{3,0,2,1:T(8,128)(2,1)}), bf16[16,1,12,1024]{3,0,2,1:T(8,128)(2,1)}) %reduce-scatter.2.cloned.1.call-update) | async-done | bytes 393232 | tf_op jit(solution)/shard_map/reduce_scatter | solution.py:132
  133.4 2.0 %copy.45 = bf16[16,1,12,1024]{3,2,1,0:T(8,128)(2,1)} copy(bf16[16,1,12,1024]{3,0,2,1:T(8,128)(2,1)} %reduce-scatter.2.cloned.1.call-done) | data formatting | bytes 786432 | tf_op jit(solution)/shard_map/reduce_scatter | solution.py:132
  135.4 6.6 %all-to-all-start.2 = ((bf16[16,1,12,1024]{3,2,1,0:T(8,128)(2,1)}), bf16[16,1,12,1024]{3,2,1,0:T(8,128)(2,1)S(1)}, u32[]{:S(2)}, u32[]{:S(2)}) async-start(bf16[16,1,12,1024]{3,2,1,0:T(8,128)(2,1)} %copy.45), calls=%async_computation.3 | async-start | bytes 1048576 | tf_op jit(solution)/shard_map/all_to_all | solution.py:135
  142.3 12.6 %all-to-all-done.2 = bf16[16,1,12,1024]{3,2,1,0:T(8,128)(2,1)S(1)} async-done(((bf16[16,1,12,1024]{3,2,1,0:T(8,128)(2,1)}), bf16[16,1,12,1024]{3,2,1,0:T(8,128)(2,1)S(1)}, u32[]{:S(2)}, u32[]{:S(2)}) %all-to-all-start.2) | async-done | bytes 393248 | tf_op jit(solution)/shard_map/all_to_all | solution.py:135
  154.9 0.3 fusion.17
  155.2 4.7 %all_gather.11 = bf16[16,2048]{1,0:T(8,128)(2,1)S(1)} all-gather(bf16[16,1024]{1,0:T(8,128)(2,1)S(1)} %add_convert_fusion), channel_id=1, replica_groups=mesh['ep'=16,'tp'=2] {'tp'}, dimensions={1}, use_global_device_ids=true | all-gather | bytes 98304 | tf_op jit(solution)/shard_map/all_gather | solution.py:149
  159.8 0.6 copy.63
  (59 shorter events, 1.9 us)
Async XLA Ops:
  7.2 8.3 %copy-start = (bf16[16,1,64,1024]{3,2,1,0:T(8,128)(2,1)S(1)}, bf16[16,1,64,1024]{3,2,1,0:T(8,128)(2,1)}, u32[]{:S(2)}) copy-start(bf16[16,1,64,1024]{3,2,1,0:T(8,128)(2,1)} %param.25) | copy-start | bytes 6291460
  7.2 68.3 %all-gather.2.cloned.1.call-start = ((), (), s32[]{:S(2)}) async-start(), calls=%async_computation.4 | async-start | bytes 1114112 | tf_op jit(solution)/shard_map/all_gather | solution.py:95
  10.4 3.3 %copy-start.2 = (bf16[16,2048]{1,0:T(8,128)(2,1)S(1)}, bf16[16,2048]{1,0:T(8,128)(2,1)}, u32[]{:S(2)}) copy-start(bf16[16,2048]{1,0:T(8,128)(2,1)} %param.18) | copy-start | bytes 196612
  10.4 4.4 %copy-start.1 = (f32[16,16,1024]{2,1,0:T(8,128)S(1)}, f32[16,16,1024]{2,1,0:T(8,128)}, u32[]{:S(2)}) copy-start(f32[16,16,1024]{2,1,0:T(8,128)} %param.27) | copy-start | bytes 3145732
  10.5 4.8 %copy-start.13 = (bf16[2048,16]{0,1:T(8,128)(2,1)S(1)}, bf16[2048,16]{0,1:T(8,128)(2,1)}, u32[]{:S(2)}) copy-start(bf16[2048,16]{0,1:T(8,128)(2,1)} %param.23) | copy-start | bytes 196612
  10.5 4.8 %copy-start.14 = (f32[16]{0:T(128)S(1)}, f32[16]{0:T(128)}, u32[]{:S(2)}) copy-start(f32[16]{0:T(128)} %param.24) | copy-start | bytes 196
  14.9 1.2 copy-start.15
  15.5 0.6 copy-start.8
  15.5 1.0 copy-start.5
  15.5 1.8 %copy-start.10 = (bf16[16,1,64,1024]{3,2,1,0:T(8,128)(2,1)S(1)}, bf16[16,1,64,1024]{3,2,1,0:T(8,128)(2,1)}, u32[]{:S(2)}) copy-start(bf16[16,1,64,1024]{3,2,1,0:T(8,128)(2,1)} %param.26) | copy-start | bytes 6291460
  17.3 2.9 %copy-start.9 = (bf16[2048]{0:T(1024)(128)(2,1)S(1)}, bf16[2048]{0:T(1024)(128)(2,1)}, u32[]{:S(2)}) copy-start(bf16[2048]{0:T(1024)(128)(2,1)} %param.30) | copy-start | bytes 12292
  17.3 2.9 %copy-start.6 = (s32[16,6]{0,1:T(8,128)S(1)}, s32[16,6]{0,1:T(8,128)}, u32[]{:S(2)}) copy-start(s32[16,6]{0,1:T(8,128)} %param.31) | copy-start | bytes 1156
  17.3 58.2 %copy-start.4 = (bf16[128,2048]{1,0:T(8,128)(2,1)S(1)}, bf16[128,2048]{1,0:T(8,128)(2,1)}, u32[]{:S(2)}) copy-start(bf16[128,2048]{1,0:T(8,128)(2,1)} %param.29) | copy-start | bytes 1572868
  77.8 10.4 %all-to-all-start = ((bf16[16,16,128]{2,1,0:T(8,128)(2,1)}), bf16[16,16,128]{2,1,0:T(8,128)(2,1)S(1)}, u32[]{:S(2)}, u32[]{:S(2)}) async-start(bf16[16,16,128]{2,1,0:T(8,128)(2,1)} %bitcast.5), calls=%async_computation | async-start | bytes 131072 | tf_op jit(solution)/shard_map/all_to_all | solution.py:100
  81.8 51.6 %reduce-scatter.2.cloned.1.call-start = ((), (), s32[]{:S(2)}) async-start(), calls=%async_computation.5 | async-start | bytes 1179648 | tf_op jit(solution)/shard_map/reduce_scatter | solution.py:132
  91.3 27.2 %copy-start.11 = (bf16[1,2048,256]{2,1,0:T(8,128)(2,1)S(1)}, bf16[1,2048,256]{2,1,0:T(8,128)(2,1)}, u32[]{:S(2)}) copy-start(bf16[1,2048,256]{2,1,0:T(8,128)(2,1)} %param.33) | copy-start | bytes 3145732
  117.5 1.0 copy-start.3
  118.5 1.2 copy-start.12
  123.2 19.0 %copy-start.7 = (f32[16,6]{0,1:T(8,128)S(1)}, f32[16,6]{0,1:T(8,128)}, u32[]{:S(2)}) copy-start(f32[16,6]{0,1:T(8,128)} %param.32) | copy-start | bytes 1156
  135.4 19.4 %all-to-all-start.2 = ((bf16[16,1,12,1024]{3,2,1,0:T(8,128)(2,1)}), bf16[16,1,12,1024]{3,2,1,0:T(8,128)(2,1)S(1)}, u32[]{:S(2)}, u32[]{:S(2)}) async-start(bf16[16,1,12,1024]{3,2,1,0:T(8,128)(2,1)} %copy.45), calls=%async_computation.3 | async-start | bytes 1048576 | tf_op jit(solution)/shard_map/all_to_all | solution.py:135
Sparse Core Ops, SparseCore 0:
  20.3 55.1 all-gather.1
  123.4 9.9 reduce-scatter.1
where the time goes:
time: 168 us; the launch traced here: 167 us
  waiting for transfers between devices  83.8 us (50%)
  blocking collectives  32.8 us (20%)
  matrix products  14.7 us (9%)
  between operations  14.3 us (9%)
  starting transfers between devices  10.7 us (6%)
  local copies, waits for them, and re-layouts  6.49 us (4%)
  other arithmetic  4.48 us (3%)
    all_gather x1, waiting for transfers between devices, per_device(): lax.all_gather(whole_heads, 'ep', axis=0, tiled=True)  54.7 us
    all_to_all x1, blocking collectives, per_device(): lax.all_to_all(outgoing, 'ep', split_axis=0, concat_axis=0, tiled=True)  26.2 us
    all_to_all x1, waiting for transfers between devices, per_device(): lax.all_to_all(half_sum, 'ep', split_axis=0, concat_axis=0, tiled=True)  12.6 us
    reduce_scatter x1, waiting for transfers between devices, per_device(): lax.psum_scatter(partial_out.astype(jnp.bfloat16), 'tp', scatter_dimensio...  10.1 us
    all_to_all x1, starting transfers between devices, per_device(): lax.all_to_all(half_sum, 'ep', split_axis=0, concat_axis=0, tiled=True)  6.63 us
    all_to_all x1, waiting for transfers between devices, per_device(): lax.all_to_all(projected, 'ep', split_axis=0, concat_axis=1, tiled=True)  6.32 us
    all_gather x1, blocking collectives, per_device(): lax.all_gather((own_part + expert_mix).astype(jnp.bfloat16), 'tp', axis=1...  4.65 us
    all_to_all x1, starting transfers between devices, per_device(): lax.all_to_all(projected, 'ep', split_axis=0, concat_axis=1, tiled=True)  4.02 us
  transfers between devices with their start and end apart: 4, of which 4 were waited for; matrix products, arithmetic and copies ran while one was open for 0% of the time, Pallas kernels for 0%

commit v1 on v0

--- a/solution.py
+++ b/solution.py
@@ -1,6 +1,10 @@
+import functools
+
 import jax
 import jax.numpy as jnp
 from jax import lax
+from jax.experimental import pallas as pl
+from jax.experimental.pallas import tpu as pltpu
 from jax.sharding import PartitionSpec as P
 
 HD = 64
@@ -16,26 +20,8 @@
     return floats * inv_root * gain.astype(jnp.float32)
 
 
-def per_device(
-    hidden,
-    attn_gain,
-    query_weight,
-    key_weight,
-    value_weight,
-    forget_weight,
-    forget_bias,
-    cache_keys,
-    cache_values,
-    cache_logsum,
-    lengths,
-    out_weight,
-    ffn_gain,
-    expert_ids,
-    expert_scores,
-    gate_weights,
-    up_weights,
-    down_weights,
-):
+def attend(hidden, attn_gain, query_weight, key_weight, value_weight, forget_weight, forget_bias,
+           cache_keys, cache_values, cache_logsum, lengths):
     rows_here = hidden.shape[0]
     query_heads = query_weight.shape[1] // HD
     key_heads = key_weight.shape[1] // HD
@@ -90,6 +76,12 @@
         * value_new.astype(jnp.float32)[:, :, None, :]
     )
     attended = attended.reshape(rows_here, query_heads * HD).astype(jnp.bfloat16)
+    return attended, key_new, value_new, new_logsum
+
+
+def rest_general(attended, hidden, out_weight, ffn_gain, expert_ids, expert_scores,
+                 gate_weights, up_weights, down_weights):
+    rows_here = hidden.shape[0]
     whole_heads = lax.all_gather(attended, "tp", axis=1, tiled=True)
     projected = lax.dot_general(
         lax.all_gather(whole_heads, "ep", axis=0, tiled=True),
@@ -147,6 +139,186 @@
         residual, lax.axis_index("tp") * share_width, share_width, 1
     )
     updated = lax.all_gather((own_part + expert_mix).astype(jnp.bfloat16), "tp", axis=1, tiled=True)
+    return updated
+
+
+MESH = pl.DeviceIdType.MESH
+
+
+def rest_body(n, att_ref, hid_ref, gain_ref, mix_ref, ow_hbm, gate_hbm, up_hbm, down_hbm, out_ref,
+              heads, ow, gate, up, down, part, part_in, proj, mixed, resid, rows, act, eout, back, upd,
+              send, recv, pair_send, pair_recv, local):
+    me, tp = lax.axis_index("ep"), lax.axis_index("tp")
+    seqs, width = hid_ref.shape
+    half = width // 2
+    feats = ow.shape[0]
+    cols = att_ref.shape[1]
+    peers = [lax.rem(me + k, n) for k in range(1, n)]
+    sources = [lax.rem(me + n - k, n) for k in range(1, n)]
+
+    def mine(i):
+        return pl.ds(pl.multiple_of(i * seqs, seqs), seqs)
+
+    my_half = pl.ds(pl.multiple_of(tp * half, half), half)
+    other_half = pl.ds(pl.multiple_of((1 - tp) * half, half), half)
+
+    def remote(src, dst, s, r, ep, core):
+        return pltpu.make_async_remote_copy(
+            src_ref=src, dst_ref=dst, send_sem=s, recv_sem=r, device_id=(ep, core), device_id_type=MESH)
+
+    loads = [
+        pltpu.make_async_copy(ow_hbm.at[:, pl.ds(pl.multiple_of(tp * cols, cols), cols)], ow, local.at[0]),
+        pltpu.make_async_copy(gate_hbm, gate, local.at[1]),
+        pltpu.make_async_copy(up_hbm, up, local.at[2]),
+        pltpu.make_async_copy(down_hbm.at[:, my_half], down.at[tp], local.at[3]),
+    ]
+    for c in loads:
+        c.start()
+    barrier = pltpu.get_barrier_semaphore()
+    for p in peers:
+        pl.semaphore_signal(barrier, inc=1, device_id=(p, tp), device_id_type=MESH)
+    pl.semaphore_signal(barrier, inc=1, device_id=(me, 1 - tp), device_id_type=MESH)
+    pl.semaphore_wait(barrier, n)
+
+    sent = []
+
+    def begin(c):
+        c.start()
+        sent.append(c)
+        return c
+
+    first = [begin(remote(att_ref, heads.at[mine(me)], send.at[0, k], recv.at[0, k], p, tp))
+             for k, p in enumerate(peers)]
+    swap_down = begin(remote(down_hbm.at[:, other_half], down.at[tp], pair_send.at[0], pair_recv.at[0], me, 1 - tp))
+    heads[mine(me), :] = att_ref[...]
+    loads[0].wait()
+    for c in first:
+        c.wait_recv()
+    part[...] = lax.dot_general(heads[...], ow[...], (((1,), (1,)), ((), ())), preferred_element_type=jnp.float32)
+    swap = begin(remote(part, part_in, pair_send.at[1], pair_recv.at[1], me, 1 - tp))
+    swap.wait_recv()
+    proj[...] = (part[...] + part_in[...]).astype(jnp.bfloat16)
+    my_feats = pl.ds(pl.multiple_of(me * feats, feats), feats)
+    second = [begin(remote(proj.at[mine(p)], mixed.at[:, my_feats], send.at[1, k], recv.at[1, k], p, tp))
+              for k, p in enumerate(peers)]
+    mixed[:, my_feats] = proj[mine(me), :]
+    for c in second:
+        c.wait_recv()
+    residual = hid_ref[...].astype(jnp.float32) + mixed[...].astype(jnp.float32)
+    resid[...] = residual
+    rows[mine(me), :] = root_norm(residual, gain_ref[...]).astype(jnp.bfloat16)
+
+    third = [begin(remote(rows.at[mine(me), my_half], rows.at[mine(me), my_half],
+                          send.at[2, k], recv.at[2, k], p, tp)) for k, p in enumerate(peers)]
+    fourth = []
+    for k, s in enumerate(sources):
+        third[k].wait_recv()
+        fourth.append(begin(remote(rows.at[mine(s), my_half], rows.at[mine(s), my_half],
+                                   send.at[3, k], recv.at[3, k], me, 1 - tp)))
+    loads[1].wait()
+    loads[2].wait()
+    for c in fourth:
+        c.wait_recv()
+    gate_act = jnp.dot(rows[...], gate[...], preferred_element_type=jnp.float32)
+    up_act = jnp.dot(rows[...], up[...], preferred_element_type=jnp.float32)
+    act[tp] = (gate_act / (1.0 + jnp.exp(-gate_act)) * up_act).astype(jnp.bfloat16)
+    swap = begin(remote(act.at[tp], act.at[tp], pair_send.at[2], pair_recv.at[2], me, 1 - tp))
+    loads[3].wait()
+    swap_down.wait_recv()
+    swap.wait_recv()
+    eout[...] = (jnp.dot(act[0], down[0], preferred_element_type=jnp.float32)
+                 + jnp.dot(act[1], down[1], preferred_element_type=jnp.float32)).astype(jnp.bfloat16)
+    fifth = [begin(remote(eout.at[mine(p)], back.at[me], send.at[4, k], recv.at[4, k], p, tp))
+             for k, p in enumerate(peers)]
+    back[me] = eout[mine(me), :]
+    for c in fifth:
+        c.wait_recv()
+    total = resid[:, my_half]
+    weights = mix_ref[...]
+    summed = jnp.zeros_like(total)
+    for e in range(n):
+        summed = summed + weights[:, e:e + 1] * back[e].astype(jnp.float32)
+    upd[:, my_half] = (total + summed).astype(jnp.bfloat16)
+    swap = begin(remote(upd.at[:, my_half], upd.at[:, my_half], pair_send.at[3], pair_recv.at[3], me, 1 - tp))
+    swap.wait_recv()
+    out_ref[...] = upd[...]
+    for c in sent:
+        c.wait_send()
+
+
+def rest_kernel(attended, hidden, out_weight, ffn_gain, expert_ids, expert_scores,
+                gate_weights, up_weights, down_weights):
+    n = lax.axis_size("ep")
+    seqs, width = hidden.shape
+    cols = attended.shape[1]
+    feats = out_weight.shape[0]
+    units = gate_weights.shape[2]
+    half = width // 2
+    route_weight = expert_scores / jnp.sum(expert_scores, axis=-1, keepdims=True)
+    lanes = -(-n // 128) * 128
+    chosen = expert_ids[:, :, None] == jnp.arange(lanes, dtype=jnp.int32)[None, None, :]
+    mix = jnp.sum(jnp.where(chosen, route_weight[:, :, None], 0.0), axis=1)
+    bf16, f32 = jnp.bfloat16, jnp.float32
+    vmem = pl.BlockSpec(memory_space=pltpu.VMEM)
+    hbm = pl.BlockSpec(memory_space=pl.ANY)
+    return pl.pallas_call(
+        functools.partial(rest_body, n),
+        out_shape=jax.ShapeDtypeStruct((seqs, width), bf16),
+        in_specs=[vmem] * 4 + [hbm] * 4,
+        out_specs=vmem,
+        scratch_shapes=[
+            pltpu.VMEM((n * seqs, cols), bf16),
+            pltpu.VMEM((feats, cols), bf16),
+            pltpu.VMEM((width, units), bf16),
+            pltpu.VMEM((width, units), bf16),
+            pltpu.VMEM((2, units, half), bf16),
+            pltpu.VMEM((n * seqs, feats), f32),
+            pltpu.VMEM((n * seqs, feats), f32),
+            pltpu.VMEM((n * seqs, feats), bf16),
+            pltpu.VMEM((seqs, width), bf16),
+            pltpu.VMEM((seqs, width), f32),
+            pltpu.VMEM((n * seqs, width), bf16),
+            pltpu.VMEM((2, n * seqs, units), bf16),
+            pltpu.VMEM((n * seqs, half), bf16),
+            pltpu.VMEM((n, seqs, half), bf16),
+            pltpu.VMEM((seqs, width), bf16),
+            pltpu.SemaphoreType.DMA((5, n)),
+            pltpu.SemaphoreType.DMA((5, n)),
+            pltpu.SemaphoreType.DMA((4,)),
+            pltpu.SemaphoreType.DMA((4,)),
+            pltpu.SemaphoreType.DMA((4,)),
+        ],
+        compiler_params=pltpu.CompilerParams(
+            collective_id=0, has_side_effects=True, vmem_limit_bytes=40 * 1024 * 1024),
+    )(attended, hidden, ffn_gain[None, :], mix, out_weight, gate_weights[0], up_weights[0], down_weights[0])
+
+
+def per_device(
+    hidden,
+    attn_gain,
+    query_weight,
+    key_weight,
+    value_weight,
+    forget_weight,
+    forget_bias,
+    cache_keys,
+    cache_values,
+    cache_logsum,
+    lengths,
+    out_weight,
+    ffn_gain,
+    expert_ids,
+    expert_scores,
+    gate_weights,
+    up_weights,
+    down_weights,
+):
+    attended, key_new, value_new, new_logsum = attend(
+        hidden, attn_gain, query_weight, key_weight, value_weight, forget_weight, forget_bias,
+        cache_keys, cache_values, cache_logsum, lengths)
+    rest = rest_kernel if out_weight.shape[0] % 128 == 0 and gate_weights.shape[0] == 1 else rest_general
+    updated = rest(attended, hidden, out_weight, ffn_gain, expert_ids, expert_scores,
+                   gate_weights, up_weights, down_weights)
     return (updated, key_new, value_new, new_logsum)
 
 

time: 168 us -> 71.7 us (0.43)
  the two profiles are of different devices: /device:TPU:1 before, /device:TPU:29 now
where the time goes in v1:
time: 71.7 us; the launch traced here: 71.4 us
  Pallas kernels  57.1 us (80%)
  matrix products  5.68 us (8%)
  local copies, waits for them, and re-layouts  5.08 us (7%)
  other arithmetic  2.61 us (4%)
  between operations  0.9 us (1%)
    pallas_call x1, Pallas kernels, rest_kernel(): pl.pallas_call(functools.partial(rest_body, n), out_shape=jax.ShapeDtypeS...  57.1 us
    unnamed x37, local copies, waits for them, and re-layouts  4.83 us
    dot_general x1, matrix products, attend(): jnp.dot(normed, query_weight, preferred_element_type=jnp.float32)  3.01 us

profile of v1, /device:TPU:29, one launch (start us, length us, event | category | flops | bytes accessed | tf_op | source)
XLA Modules:
  0.0 71.4 jit_solution(4919650069964225986)
XLA Ops:
  0.6 0.0 copy-start
  0.6 0.8 %convert_element_type.41 = f32[2048]{0:T(1024)S(1)} convert(bf16[2048]{0:T(1024)(128)(2,1)} %param.19) | non-fusion elementwise | flops 2048 | bytes 12288 | tf_op jit(solution)/shard_map/convert_element_type | solution.py:20
  1.5 1.0 %fusion.26 = f32[16]{0:T(128)S(1)} fusion(bf16[16,2048]{1,0:T(8,128)(2,1)} %hid_ref.1), kind=kLoop, calls=%fused_computation.23 | loop fusion | flops 98288 | bytes 65600 | tf_op jit(solution)/shard_map/reduce_sum | solution.py:19
  2.5 0.0 copy-start.6
  2.5 0.0 copy-start.1
  2.5 0.0 copy-start.15
  2.5 0.0 copy-start.16
  2.5 3.0 %convolution_convert_fusion = bf16[16,1024]{1,0:T(8,128)(2,1)S(1)} fusion(bf16[2048,1024]{1,0:T(8,128)(2,1)} %param.20, bf16[16,2048]{1,0:T(8,128)(2,1)} %hid_ref.1, f32[2048]{0:T(1024)S(1)} %convert_element_type.41, f32[16]{0:T(128)S(1)} %add_rsqrt_fusion), kind=kOutput, calls=%fused_computation.10 | convolution fusion | flops 67256320 | bytes 4300864 | tf_op jit(solution)/shard_map/dot_general | solution.py:32
  5.5 0.1 reshape.123
  5.7 0.1 iota_compare_fusion
  5.8 0.2 select_reduce_fusion
  6.0 0.2 fusion.30
  6.2 0.0 copy-start.9
  6.2 0.1 iota_compare_fusion.1
  6.3 0.0 copy-start.7
  6.3 0.0 copy-start.13
  6.4 0.5 fusion.39
  6.9 0.4 copy-done.14
  7.3 0.2 convolution_convert_fusion.2
  7.5 0.2 fusion.31
  7.7 0.3 fusion.23
  8.0 0.8 %fusion.40 = (f32[16,64]{1,0:T(8,128)S(1)}, bf16[16,64]{1,0:T(8,128)(2,1)}) fusion(bf16[2048,64]{0,1:T(8,128)(2,1)S(1)} %copy-done.7, bf16[16,2048]{1,0:T(8,128)(2,1)S(1)} %copy-done.1, f32[2048]{0:T(1024)S(1)} %convert_element_type.41, f32[16]{0:T(128)S(1)} %add_rsqrt_fusion), kind=kOutput, calls=%fused_computation.44 | convolution fusion | flops 4327424 | bytes 342080 | tf_op jit(solution)/shard_map/dot_general | solution.py:39
  8.9 0.7 fusion.19
  9.6 0.0 copy-done.17
  9.6 0.1 convert_element_type.51.att_ref
  9.8 0.1 select_reduce_fusion.1.mix_ref
  9.9 0.2 copy-done.2
  10.1 1.2 %copy-done.3 = bf16[1,2048,256]{2,1,0:T(8,128)(2,1)S(1)} copy-done((bf16[1,2048,256]{2,1,0:T(8,128)(2,1)S(1)}, bf16[1,2048,256]{2,1,0:T(8,128)(2,1)}, u32[]{:S(2)}) %copy-start.3) | copy-done | bytes 1048600
  11.4 1.2 %copy-done.4 = bf16[1,256,2048]{2,1,0:T(8,128)(2,1)S(1)} copy-done((bf16[1,256,2048]{2,1,0:T(8,128)(2,1)S(1)}, bf16[1,256,2048]{2,1,0:T(8,128)(2,1)}, u32[]{:S(2)}) %copy-start.4) | copy-done | bytes 1048600
  12.6 1.0 %copy-done.5 = bf16[128,2048]{1,0:T(8,128)(2,1)S(1)} copy-done((bf16[128,2048]{1,0:T(8,128)(2,1)S(1)}, bf16[128,2048]{1,0:T(8,128)(2,1)}, u32[]{:S(2)}) %copy-start.5) | copy-done | bytes 524312
  13.6 57.1 %shard_map.201 = bf16[16,2048]{1,0:T(8,128)(2,1)S(1)} custom-call(bf16[16,1024]{1,0:T(8,128)(2,1)S(1)} %convert_element_type.51.att_ref, bf16[16,2048]{1,0:T(8,128)(2,1)S(1)} %copy-done.1, bf16[1,2048]{1,0:T(2,128)(2,1)S(1)} %broadcast_in_dim.56.gain_ref, f32[16,128]{1,0:T(8,128)S(1)} %select_reduce_fusion.1.mix_ref, bf16[128,2048]{1,0:T(8,128)(2,1)S(1)} %copy-done.5, ...), custom_call_target="tpu_custom_call" | custom-call | tf_op jit(solution)/shard_map/pallas_call | solution.py:264
  70.7 0.6 copy.29
  (29 shorter events, 0.1 us)
Async XLA Ops:
  0.6 5.7 %copy-start = (bf16[16,1,64,1024]{3,2,1,0:T(8,128)(2,1)S(1)}, bf16[16,1,64,1024]{3,2,1,0:T(8,128)(2,1)}, u32[]{:S(2)}) copy-start(bf16[16,1,64,1024]{3,2,1,0:T(8,128)(2,1)} %param.25) | copy-start | bytes 6291460
  2.5 3.2 %copy-start.12 = (s32[16]{0:T(128)S(1)}, s32[16]{0:T(128)}, u32[]{:S(2)}) copy-start(s32[16]{0:T(128)} %param.28) | copy-start | bytes 196
  2.5 3.3 %copy-start.6 = (f32[16,16,1024]{2,1,0:T(8,128)S(1)}, f32[16,16,1024]{2,1,0:T(8,128)}, u32[]{:S(2)}) copy-start(f32[16,16,1024]{2,1,0:T(8,128)} %param.27) | copy-start | bytes 3145732
  2.5 3.5 %copy-start.1 = (bf16[16,2048]{1,0:T(8,128)(2,1)S(1)}, bf16[16,2048]{1,0:T(8,128)(2,1)}, u32[]{:S(2)}) copy-start(bf16[16,2048]{1,0:T(8,128)(2,1)} %hid_ref.1) | copy-start | bytes 196612
  2.5 3.5 %copy-start.15 = (bf16[2048,16]{0,1:T(8,128)(2,1)S(1)}, bf16[2048,16]{0,1:T(8,128)(2,1)}, u32[]{:S(2)}) copy-start(bf16[2048,16]{0,1:T(8,128)(2,1)} %param.23) | copy-start | bytes 196612
  2.5 3.5 %copy-start.16 = (f32[16]{0:T(128)S(1)}, f32[16]{0:T(128)}, u32[]{:S(2)}) copy-start(f32[16]{0:T(128)} %param.24) | copy-start | bytes 196
  6.2 0.7 copy-start.9
  6.3 1.0 %copy-start.14 = (bf16[2048,64]{0,1:T(8,128)(2,1)S(1)}, bf16[2048,64]{0,1:T(8,128)(2,1)}, u32[]{:S(2)}) copy-start(bf16[2048,64]{0,1:T(8,128)(2,1)} %param.21) | copy-start | bytes 786436
  6.3 1.7 %copy-start.7 = (bf16[2048,64]{0,1:T(8,128)(2,1)S(1)}, bf16[2048,64]{0,1:T(8,128)(2,1)}, u32[]{:S(2)}) copy-start(bf16[2048,64]{0,1:T(8,128)(2,1)} %param.22) | copy-start | bytes 786436
  6.3 2.5 %copy-start.13 = (bf16[16,1,64,1024]{3,2,1,0:T(8,128)(2,1)S(1)}, bf16[16,1,64,1024]{3,2,1,0:T(8,128)(2,1)}, u32[]{:S(2)}) copy-start(bf16[16,1,64,1024]{3,2,1,0:T(8,128)(2,1)} %param.26) | copy-start | bytes 6291460
  7.5 2.1 %copy-start.17 = (bf16[16,64]{1,0:T(8,128)(2,1)}, bf16[16,64]{1,0:T(8,128)(2,1)S(1)}, u32[]{:S(2)}) copy-start(bf16[16,64]{1,0:T(8,128)(2,1)S(1)} %convolution_convert_fusion.2) | copy-start | bytes 6148
  8.9 0.9 %copy-start.8 = (f32[16,6]{0,1:T(8,128)S(1)}, f32[16,6]{0,1:T(8,128)}, u32[]{:S(2)}) copy-start(f32[16,6]{0,1:T(8,128)} %param.32) | copy-start | bytes 1156
  8.9 0.9 %copy-start.11 = (s32[16,6]{0,1:T(8,128)S(1)}, s32[16,6]{0,1:T(8,128)}, u32[]{:S(2)}) copy-start(s32[16,6]{0,1:T(8,128)} %param.31) | copy-start | bytes 1156
  8.9 1.0 %copy-start.10 = (bf16[2048]{0:T(1024)(128)(2,1)S(1)}, bf16[2048]{0:T(1024)(128)(2,1)}, u32[]{:S(2)}) copy-start(bf16[2048]{0:T(1024)(128)(2,1)} %param.30) | copy-start | bytes 12292
  8.9 1.3 %copy-start.2 = (bf16[1,2048,256]{2,1,0:T(8,128)(2,1)S(1)}, bf16[1,2048,256]{2,1,0:T(8,128)(2,1)}, u32[]{:S(2)}) copy-start(bf16[1,2048,256]{2,1,0:T(8,128)(2,1)} %param.33) | copy-start | bytes 3145732
  10.1 1.2 %copy-start.3 = (bf16[1,2048,256]{2,1,0:T(8,128)(2,1)S(1)}, bf16[1,2048,256]{2,1,0:T(8,128)(2,1)}, u32[]{:S(2)}) copy-start(bf16[1,2048,256]{2,1,0:T(8,128)(2,1)} %param.34) | copy-start | bytes 3145732
  11.4 1.2 %copy-start.4 = (bf16[1,256,2048]{2,1,0:T(8,128)(2,1)S(1)}, bf16[1,256,2048]{2,1,0:T(8,128)(2,1)}, u32[]{:S(2)}) copy-start(bf16[1,256,2048]{2,1,0:T(8,128)(2,1)} %param.35) | copy-start | bytes 3145732
  12.6 1.0 %copy-start.5 = (bf16[128,2048]{1,0:T(8,128)(2,1)S(1)}, bf16[128,2048]{1,0:T(8,128)(2,1)}, u32[]{:S(2)}) copy-start(bf16[128,2048]{1,0:T(8,128)(2,1)} %ow_hbm.1) | copy-start | bytes 1572868

commit v2 on v1

--- a/solution.py
+++ b/solution.py
@@ -1,4 +1,5 @@
 import functools
+import math
 
 import jax
 import jax.numpy as jnp
@@ -146,15 +147,21 @@
 
 
 def rest_body(n, att_ref, hid_ref, gain_ref, mix_ref, ow_hbm, gate_hbm, up_hbm, down_hbm, out_ref,
-              heads, ow, gate, up, down, part, part_in, proj, mixed, resid, rows, act, eout, back, upd,
+              heads, ow, gate, up, down, part, part_in, proj, mixed, resid, rows, act, eout, back, sums, mix, upd,
               send, recv, pair_send, pair_recv, local):
     me, tp = lax.axis_index("ep"), lax.axis_index("tp")
     seqs, width = hid_ref.shape
     half = width // 2
     feats = ow.shape[0]
     cols = att_ref.shape[1]
+    inner = math.isqrt(n)
+    outer = n // inner
+    line, spot = me // inner, lax.rem(me, inner)
+
+    def there(dl, ds):
+        return lax.rem(line + dl + outer, outer) * inner + lax.rem(spot + ds + inner, inner)
+
     peers = [lax.rem(me + k, n) for k in range(1, n)]
-    sources = [lax.rem(me + n - k, n) for k in range(1, n)]
 
     def mine(i):
         return pl.ds(pl.multiple_of(i * seqs, seqs), seqs)
@@ -187,13 +194,33 @@
         sent.append(c)
         return c
 
-    first = [begin(remote(att_ref, heads.at[mine(me)], send.at[0, k], recv.at[0, k], p, tp))
+    def gather(own, view, phase, use):
+        far = {dl: begin(remote(own, view(me), send.at[phase, dl * inner], recv.at[phase, dl * inner],
+                                there(dl, 0), tp)) for dl in range(1, outer)}
+        near = []
+        for dl in range(outer):
+            source = there(-dl, 0)
+            if dl:
+                far[dl].wait_recv()
+            block = view(source) if dl else own
+            for ds in range(1, inner):
+                near.append((there(-dl, -ds), begin(remote(
+                    block, view(source), send.at[phase, dl * inner + ds], recv.at[phase, dl * inner + ds],
+                    there(0, ds), tp))))
+            if dl:
+                use(dl * inner, source)
+        for k, (source, c) in enumerate(near):
+            c.wait_recv()
+            use(k // (inner - 1) * inner + k % (inner - 1) + 1, source)
+
+    swap_down = remote(down_hbm.at[:, other_half], down.at[tp], pair_send.at[0], pair_recv.at[0], me, 1 - tp)
+    begin(swap_down)
+    heads[mine(me), :] = att_ref[...]
+    gather(att_ref, lambda s: heads.at[mine(s)], 0, lambda k, s: None)
+    gains = [begin(remote(mix_ref.at[p], mix.at[me], send.at[5, k], recv.at[5, k], p, tp))
              for k, p in enumerate(peers)]
-    swap_down = begin(remote(down_hbm.at[:, other_half], down.at[tp], pair_send.at[0], pair_recv.at[0], me, 1 - tp))
-    heads[mine(me), :] = att_ref[...]
+    mix[me] = mix_ref[me]
     loads[0].wait()
-    for c in first:
-        c.wait_recv()
     part[...] = lax.dot_general(heads[...], ow[...], (((1,), (1,)), ((), ())), preferred_element_type=jnp.float32)
     swap = begin(remote(part, part_in, pair_send.at[1], pair_recv.at[1], me, 1 - tp))
     swap.wait_recv()
@@ -208,13 +235,13 @@
     resid[...] = residual
     rows[mine(me), :] = root_norm(residual, gain_ref[...]).astype(jnp.bfloat16)
 
-    third = [begin(remote(rows.at[mine(me), my_half], rows.at[mine(me), my_half],
-                          send.at[2, k], recv.at[2, k], p, tp)) for k, p in enumerate(peers)]
     fourth = []
-    for k, s in enumerate(sources):
-        third[k].wait_recv()
+
+    def pass_on(k, s):
         fourth.append(begin(remote(rows.at[mine(s), my_half], rows.at[mine(s), my_half],
                                    send.at[3, k], recv.at[3, k], me, 1 - tp)))
+
+    gather(rows.at[mine(me), my_half], lambda s: rows.at[mine(s), my_half], 2, pass_on)
     loads[1].wait()
     loads[2].wait()
     for c in fourth:
@@ -226,18 +253,31 @@
     loads[3].wait()
     swap_down.wait_recv()
     swap.wait_recv()
-    eout[...] = (jnp.dot(act[0], down[0], preferred_element_type=jnp.float32)
-                 + jnp.dot(act[1], down[1], preferred_element_type=jnp.float32)).astype(jnp.bfloat16)
-    fifth = [begin(remote(eout.at[mine(p)], back.at[me], send.at[4, k], recv.at[4, k], p, tp))
-             for k, p in enumerate(peers)]
-    back[me] = eout[mine(me), :]
-    for c in fifth:
+    for c in gains:
         c.wait_recv()
+    eout[...] = ((jnp.dot(act[0], down[0], preferred_element_type=jnp.float32)
+                  + jnp.dot(act[1], down[1], preferred_element_type=jnp.float32))
+                 * mix[...].reshape(n * seqs, mix.shape[2])[:, :1]).astype(jnp.bfloat16)
+    near = {}
+    for dl in [d for d in range(1, outer)] + [0]:
+        for ds in range(1, inner):
+            k = dl * inner + ds
+            near[k] = begin(remote(eout.at[mine(there(dl, ds))], back.at[k], send.at[4, k], recv.at[4, k],
+                                   there(0, ds), tp))
+    far = []
+    for dl in [d for d in range(1, outer)] + [0]:
+        summed = eout[mine(there(dl, 0)), :].astype(jnp.float32)
+        for ds in range(1, inner):
+            near[dl * inner + ds].wait_recv()
+            summed = summed + back[dl * inner + ds].astype(jnp.float32)
+        if dl:
+            sums[dl] = summed.astype(jnp.bfloat16)
+            far.append((dl, begin(remote(sums.at[dl], back.at[dl * inner], send.at[4, dl * inner],
+                                         recv.at[4, dl * inner], there(dl, 0), tp))))
+    for dl, c in far:
+        c.wait_recv()
+        summed = summed + back[dl * inner].astype(jnp.float32)
     total = resid[:, my_half]
-    weights = mix_ref[...]
-    summed = jnp.zeros_like(total)
-    for e in range(n):
-        summed = summed + weights[:, e:e + 1] * back[e].astype(jnp.float32)
     upd[:, my_half] = (total + summed).astype(jnp.bfloat16)
     swap = begin(remote(upd.at[:, my_half], upd.at[:, my_half], pair_send.at[3], pair_recv.at[3], me, 1 - tp))
     swap.wait_recv()
@@ -255,9 +295,9 @@
     units = gate_weights.shape[2]
     half = width // 2
     route_weight = expert_scores / jnp.sum(expert_scores, axis=-1, keepdims=True)
-    lanes = -(-n // 128) * 128
-    chosen = expert_ids[:, :, None] == jnp.arange(lanes, dtype=jnp.int32)[None, None, :]
-    mix = jnp.sum(jnp.where(chosen, route_weight[:, :, None], 0.0), axis=1)
+    chosen = expert_ids[None, :, :] == jnp.arange(n, dtype=jnp.int32)[:, None, None]
+    mix = jnp.sum(jnp.where(chosen, route_weight[None, :, :], 0.0), axis=-1, keepdims=True)
+    mix = jnp.broadcast_to(mix, (n, seqs, 128))
     bf16, f32 = jnp.bfloat16, jnp.float32
     vmem = pl.BlockSpec(memory_space=pltpu.VMEM)
     hbm = pl.BlockSpec(memory_space=pl.ANY)
@@ -281,15 +321,17 @@
             pltpu.VMEM((2, n * seqs, units), bf16),
             pltpu.VMEM((n * seqs, half), bf16),
             pltpu.VMEM((n, seqs, half), bf16),
+            pltpu.VMEM((math.isqrt(n), seqs, half), bf16),
+            pltpu.VMEM((n, seqs, 128), f32),
             pltpu.VMEM((seqs, width), bf16),
-            pltpu.SemaphoreType.DMA((5, n)),
-            pltpu.SemaphoreType.DMA((5, n)),
+            pltpu.SemaphoreType.DMA((6, n)),
+            pltpu.SemaphoreType.DMA((6, n)),
             pltpu.SemaphoreType.DMA((4,)),
             pltpu.SemaphoreType.DMA((4,)),
             pltpu.SemaphoreType.DMA((4,)),
         ],
         compiler_params=pltpu.CompilerParams(
-            collective_id=0, has_side_effects=True, vmem_limit_bytes=40 * 1024 * 1024),
+            collective_id=0, has_side_effects=True, vmem_limit_bytes=60 * 1024 * 1024),
     )(attended, hidden, ffn_gain[None, :], mix, out_weight, gate_weights[0], up_weights[0], down_weights[0])
 
 
@@ -316,7 +358,9 @@
     attended, key_new, value_new, new_logsum = attend(
         hidden, attn_gain, query_weight, key_weight, value_weight, forget_weight, forget_bias,
         cache_keys, cache_values, cache_logsum, lengths)
-    rest = rest_kernel if out_weight.shape[0] % 128 == 0 and gate_weights.shape[0] == 1 else rest_general
+    n = lax.axis_size("ep")
+    square = math.isqrt(n) ** 2 == n
+    rest = rest_kernel if out_weight.shape[0] % 128 == 0 and gate_weights.shape[0] == 1 and square else rest_general
     updated = rest(attended, hidden, out_weight, ffn_gain, expert_ids, expert_scores,
                    gate_weights, up_weights, down_weights)
     return (updated, key_new, value_new, new_logsum)

time: 71.7 us -> 61.5 us (0.86)
  the two profiles are of different devices: /device:TPU:29 before, /device:TPU:1 now
where the time goes in v2:
time: 61.5 us; the launch traced here: 61.2 us
  Pallas kernels  48 us (78%)
  matrix products  5.67 us (9%)
  local copies, waits for them, and re-layouts  4.14 us (7%)
  other arithmetic  2.54 us (4%)
  between operations  0.86 us (1%)
    pallas_call x1, Pallas kernels, rest_kernel(): pl.pallas_call(functools.partial(rest_body, n), out_shape=jax.ShapeDtypeS...  48 us
    dot_general x1, matrix products, attend(): jnp.dot(normed, query_weight, preferred_element_type=jnp.float32)  3.01 us
    unnamed x29, local copies, waits for them, and re-layouts  1.95 us

profile of v2, /device:TPU:1, one launch (start us, length us, event | category | flops | bytes accessed | tf_op | source)
XLA Modules:
  0.0 61.2 jit_solution(3490763282453629808)
XLA Ops:
  0.6 0.0 copy-start
  0.6 0.8 %convert_element_type.41 = f32[2048]{0:T(1024)S(1)} convert(bf16[2048]{0:T(1024)(128)(2,1)} %param.19) | non-fusion elementwise | flops 2048 | bytes 12288 | tf_op jit(solution)/shard_map/convert_element_type | solution.py:21
  1.5 1.0 %fusion.26 = f32[16]{0:T(128)S(1)} fusion(bf16[16,2048]{1,0:T(8,128)(2,1)} %hid_ref.1), kind=kLoop, calls=%fused_computation.23 | loop fusion | flops 98288 | bytes 65600 | tf_op jit(solution)/shard_map/reduce_sum | solution.py:20
  2.5 0.0 copy-start.1
  2.5 0.0 copy-start.2
  2.5 0.0 copy-start.11
  2.5 0.0 copy-start.12
  2.5 3.0 %convolution_convert_fusion = bf16[16,1024]{1,0:T(8,128)(2,1)S(1)} fusion(bf16[2048,1024]{1,0:T(8,128)(2,1)} %param.20, bf16[16,2048]{1,0:T(8,128)(2,1)} %hid_ref.1, f32[2048]{0:T(1024)S(1)} %convert_element_type.41, f32[16]{0:T(128)S(1)} %add_rsqrt_fusion), kind=kOutput, calls=%fused_computation.10 | convolution fusion | flops 67256320 | bytes 4300864 | tf_op jit(solution)/shard_map/dot_general | solution.py:33
  5.5 0.1 reshape.124
  5.7 0.1 iota_compare_fusion
  5.8 0.2 select_reduce_fusion
  6.0 0.2 fusion.30
  6.2 0.0 copy-start.5
  6.2 0.1 iota_compare_fusion.1
  6.3 0.0 copy-start.10
  6.3 0.0 copy-start.3
  6.3 0.0 copy-start.9
  6.4 0.5 fusion.39
  6.9 0.4 copy-done.10
  7.3 0.2 convolution_convert_fusion.2
  7.5 0.2 fusion.31
  7.7 0.3 fusion.23
  8.0 0.8 %fusion.40 = (f32[16,64]{1,0:T(8,128)S(1)}, bf16[16,64]{1,0:T(8,128)(2,1)}) fusion(bf16[2048,64]{0,1:T(8,128)(2,1)S(1)} %copy-done.3, bf16[16,2048]{1,0:T(8,128)(2,1)S(1)} %copy-done.2, f32[2048]{0:T(1024)S(1)} %convert_element_type.41, f32[16]{0:T(128)S(1)} %add_rsqrt_fusion), kind=kOutput, calls=%fused_computation.44 | convolution fusion | flops 4327424 | bytes 342080 | tf_op jit(solution)/shard_map/dot_general | solution.py:40
  8.9 0.0 copy-done.9
  8.9 0.7 %fusion.19 = bf16[16,16,64]{2,1,0:T(8,128)(2,1)S(1)} fusion(bf16[16,1,64,1024]{3,2,1,0:T(8,128)(2,1)S(1)} %copy-done.9, f32[16,16,1024]{2,1,0:T(8,128)S(1)} %get-tuple-element.7, f32[16,16]{1,0:T(8,128)S(1)} %get-tuple-element.5, f32[16,16]{1,0:T(8,128)S(1)} %multiply_maximum_fusion, f32[16,64]{1,0:T(8,128)S(1)} %get-tuple-element.8, ...), kind=kOutput, calls=%fused_computation.9 | convolution fusion | flops 34390016 | bytes 3185664 | tf_op jit(solution)/shard_map/sgjp,sgdp->sgjd/dot_general | solution.py:68
  9.6 0.0 copy-done.13
  9.6 0.7 %convert_element_type.51.att_ref = bf16[16,1024]{1,0:T(8,128)(2,1)} reshape(bf16[16,16,64]{2,1,0:T(8,128)(2,1)S(1)} %fusion.19) | data formatting | bytes 65536 | tf_op jit(solution)/shard_map/convert_element_type | solution.py:79
  10.3 0.0 copy-done.4
  10.4 0.7 %broadcast_in_dim.65.mix_ref = f32[16,16,128]{2,1,0:T(8,128)} broadcast(f32[16,16]{1,0:T(8,128)S(1)} %select_reduce_fusion.1), dimensions={0,1} | broadcast | bytes 132096 | tf_op jit(solution)/shard_map/broadcast_in_dim | solution.py:300
  11.1 0.6 broadcast_in_dim.62.gain_ref
  11.7 48.0 %shard_map.201 = bf16[16,2048]{1,0:T(8,128)(2,1)} custom-call(bf16[16,1024]{1,0:T(8,128)(2,1)} %convert_element_type.51.att_ref, bf16[16,2048]{1,0:T(8,128)(2,1)} %hid_ref.1, bf16[1,2048]{1,0:T(2,128)(2,1)} %broadcast_in_dim.62.gain_ref, f32[16,16,128]{2,1,0:T(8,128)} %broadcast_in_dim.65.mix_ref, bf16[128,2048]{1,0:T(8,128)(2,1)} %ow_hbm.1, ...), custom_call_target="tpu_custom_call" | custom-call | tf_op jit(solution)/shard_map/pallas_call | solution.py:304
  59.8 1.5 %copy.29 = bf16[16,2048]{1,0:T(8,128)(2,1)} copy(bf16[16,2048]{1,0:T(8,128)(2,1)} %shard_map.201) | data formatting | bytes 131072
  (22 shorter events, 0.1 us)
Async XLA Ops:
  0.6 5.7 %copy-start = (bf16[16,1,64,1024]{3,2,1,0:T(8,128)(2,1)S(1)}, bf16[16,1,64,1024]{3,2,1,0:T(8,128)(2,1)}, u32[]{:S(2)}) copy-start(bf16[16,1,64,1024]{3,2,1,0:T(8,128)(2,1)} %param.25) | copy-start | bytes 6291460
  2.5 3.2 %copy-start.8 = (s32[16]{0:T(128)S(1)}, s32[16]{0:T(128)}, u32[]{:S(2)}) copy-start(s32[16]{0:T(128)} %param.28) | copy-start | bytes 196
  2.5 3.3 %copy-start.1 = (f32[16,16,1024]{2,1,0:T(8,128)S(1)}, f32[16,16,1024]{2,1,0:T(8,128)}, u32[]{:S(2)}) copy-start(f32[16,16,1024]{2,1,0:T(8,128)} %param.27) | copy-start | bytes 3145732
  2.5 3.5 %copy-start.2 = (bf16[16,2048]{1,0:T(8,128)(2,1)S(1)}, bf16[16,2048]{1,0:T(8,128)(2,1)}, u32[]{:S(2)}) copy-start(bf16[16,2048]{1,0:T(8,128)(2,1)} %hid_ref.1) | copy-start | bytes 196612
  2.5 3.5 %copy-start.11 = (bf16[2048,16]{0,1:T(8,128)(2,1)S(1)}, bf16[2048,16]{0,1:T(8,128)(2,1)}, u32[]{:S(2)}) copy-start(bf16[2048,16]{0,1:T(8,128)(2,1)} %param.23) | copy-start | bytes 196612
  2.5 3.5 %copy-start.12 = (f32[16]{0:T(128)S(1)}, f32[16]{0:T(128)}, u32[]{:S(2)}) copy-start(f32[16]{0:T(128)} %param.24) | copy-start | bytes 196
  6.2 0.7 %copy-start.5 = (f32[16,16]{1,0:T(8,128)}, f32[16,16]{1,0:T(8,128)S(1)}, u32[]{:S(2)}) copy-start(f32[16,16]{1,0:T(8,128)S(1)} %fusion.30) | copy-start | bytes 3076
  6.3 1.0 %copy-start.10 = (bf16[2048,64]{0,1:T(8,128)(2,1)S(1)}, bf16[2048,64]{0,1:T(8,128)(2,1)}, u32[]{:S(2)}) copy-start(bf16[2048,64]{0,1:T(8,128)(2,1)} %param.21) | copy-start | bytes 786436
  6.3 1.7 %copy-start.3 = (bf16[2048,64]{0,1:T(8,128)(2,1)S(1)}, bf16[2048,64]{0,1:T(8,128)(2,1)}, u32[]{:S(2)}) copy-start(bf16[2048,64]{0,1:T(8,128)(2,1)} %param.22) | copy-start | bytes 786436
  6.3 2.5 %copy-start.9 = (bf16[16,1,64,1024]{3,2,1,0:T(8,128)(2,1)S(1)}, bf16[16,1,64,1024]{3,2,1,0:T(8,128)(2,1)}, u32[]{:S(2)}) copy-start(bf16[16,1,64,1024]{3,2,1,0:T(8,128)(2,1)} %param.26) | copy-start | bytes 6291460
  7.5 2.1 %copy-start.13 = (bf16[16,64]{1,0:T(8,128)(2,1)}, bf16[16,64]{1,0:T(8,128)(2,1)S(1)}, u32[]{:S(2)}) copy-start(bf16[16,64]{1,0:T(8,128)(2,1)S(1)} %convolution_convert_fusion.2) | copy-start | bytes 6148
  8.9 1.5 %copy-start.4 = (f32[16,6]{0,1:T(8,128)S(1)}, f32[16,6]{0,1:T(8,128)}, u32[]{:S(2)}) copy-start(f32[16,6]{0,1:T(8,128)} %param.32) | copy-start | bytes 1156
  8.9 1.5 %copy-start.7 = (s32[16,6]{0,1:T(8,128)S(1)}, s32[16,6]{0,1:T(8,128)}, u32[]{:S(2)}) copy-start(s32[16,6]{0,1:T(8,128)} %param.31) | copy-start | bytes 1156
  8.9 2.3 %copy-start.6 = (bf16[2048]{0:T(1024)(128)(2,1)S(1)}, bf16[2048]{0:T(1024)(128)(2,1)}, u32[]{:S(2)}) copy-start(bf16[2048]{0:T(1024)(128)(2,1)} %param.30) | copy-start | bytes 12292

commit v3 on v2

--- a/solution.py
+++ b/solution.py
@@ -197,30 +197,31 @@
     def gather(own, view, phase, use):
         far = {dl: begin(remote(own, view(me), send.at[phase, dl * inner], recv.at[phase, dl * inner],
                                 there(dl, 0), tp)) for dl in range(1, outer)}
-        near = []
+        near = [[] for _ in range(outer)]
         for dl in range(outer):
             source = there(-dl, 0)
             if dl:
                 far[dl].wait_recv()
             block = view(source) if dl else own
             for ds in range(1, inner):
-                near.append((there(-dl, -ds), begin(remote(
+                near[dl].append((dl * inner + ds, there(-dl, -ds), begin(remote(
                     block, view(source), send.at[phase, dl * inner + ds], recv.at[phase, dl * inner + ds],
                     there(0, ds), tp))))
             if dl:
                 use(dl * inner, source)
-        for k, (source, c) in enumerate(near):
-            c.wait_recv()
-            use(k // (inner - 1) * inner + k % (inner - 1) + 1, source)
+        return near
 
     swap_down = remote(down_hbm.at[:, other_half], down.at[tp], pair_send.at[0], pair_recv.at[0], me, 1 - tp)
     begin(swap_down)
     heads[mine(me), :] = att_ref[...]
-    gather(att_ref, lambda s: heads.at[mine(s)], 0, lambda k, s: None)
+    arriving = gather(att_ref, lambda s: heads.at[mine(s)], 0, lambda k, s: None)
     gains = [begin(remote(mix_ref.at[p], mix.at[me], send.at[5, k], recv.at[5, k], p, tp))
              for k, p in enumerate(peers)]
     mix[me] = mix_ref[me]
     loads[0].wait()
+    for group in arriving:
+        for _, _, c in group:
+            c.wait_recv()
     part[...] = lax.dot_general(heads[...], ow[...], (((1,), (1,)), ((), ())), preferred_element_type=jnp.float32)
     swap = begin(remote(part, part_in, pair_send.at[1], pair_recv.at[1], me, 1 - tp))
     swap.wait_recv()
@@ -235,37 +236,55 @@
     resid[...] = residual
     rows[mine(me), :] = root_norm(residual, gain_ref[...]).astype(jnp.bfloat16)
 
-    fourth = []
+    fourth = [[] for _ in range(outer)]
 
     def pass_on(k, s):
-        fourth.append(begin(remote(rows.at[mine(s), my_half], rows.at[mine(s), my_half],
+        fourth[k // inner].append(begin(remote(rows.at[mine(s), my_half], rows.at[mine(s), my_half],
                                    send.at[3, k], recv.at[3, k], me, 1 - tp)))
 
-    gather(rows.at[mine(me), my_half], lambda s: rows.at[mine(s), my_half], 2, pass_on)
-    loads[1].wait()
-    loads[2].wait()
-    for c in fourth:
-        c.wait_recv()
-    gate_act = jnp.dot(rows[...], gate[...], preferred_element_type=jnp.float32)
-    up_act = jnp.dot(rows[...], up[...], preferred_element_type=jnp.float32)
-    act[tp] = (gate_act / (1.0 + jnp.exp(-gate_act)) * up_act).astype(jnp.bfloat16)
-    swap = begin(remote(act.at[tp], act.at[tp], pair_send.at[2], pair_recv.at[2], me, 1 - tp))
-    loads[3].wait()
-    swap_down.wait_recv()
-    swap.wait_recv()
-    for c in gains:
-        c.wait_recv()
-    eout[...] = ((jnp.dot(act[0], down[0], preferred_element_type=jnp.float32)
-                  + jnp.dot(act[1], down[1], preferred_element_type=jnp.float32))
-                 * mix[...].reshape(n * seqs, mix.shape[2])[:, :1]).astype(jnp.bfloat16)
-    near = {}
-    for dl in [d for d in range(1, outer)] + [0]:
-        for ds in range(1, inner):
-            k = dl * inner + ds
-            near[k] = begin(remote(eout.at[mine(there(dl, ds))], back.at[k], send.at[4, k], recv.at[4, k],
-                                   there(0, ds), tp))
+    arriving = gather(rows.at[mine(me), my_half], lambda s: rows.at[mine(s), my_half], 2, pass_on)
+    near, swaps = {}, {}
+
+    def some(dl):
+        size = inner * seqs
+        return pl.ds(pl.multiple_of(lax.rem(line - dl + outer, outer) * size, size), size)
+
+    for step in range(outer + 2):
+        if step < outer:
+            for k, source, c in arriving[step]:
+                c.wait_recv()
+                pass_on(k, source)
+        if step == 0:
+            loads[1].wait()
+            loads[2].wait()
+            loads[3].wait()
+            swap_down.wait_recv()
+            for c in gains:
+                c.wait_recv()
+        dl = step - 1
+        if 0 <= dl < outer:
+            for c in fourth[dl]:
+                c.wait_recv()
+            block = rows[some(dl), :]
+            gate_act = jnp.dot(block, gate[...], preferred_element_type=jnp.float32)
+            up_act = jnp.dot(block, up[...], preferred_element_type=jnp.float32)
+            act[tp, some(dl), :] = (gate_act / (1.0 + jnp.exp(-gate_act)) * up_act).astype(jnp.bfloat16)
+            swaps[dl] = begin(remote(act.at[tp, some(dl)], act.at[tp, some(dl)],
+                                     pair_send.at[4 + dl], pair_recv.at[4 + dl], me, 1 - tp))
+        dl = step - 2
+        if dl >= 0:
+            swaps[dl].wait_recv()
+            weight = mix[pl.ds(lax.rem(line - dl + outer, outer) * inner, inner)]
+            eout[some(dl), :] = ((jnp.dot(act[0, some(dl), :], down[0], preferred_element_type=jnp.float32)
+                                  + jnp.dot(act[1, some(dl), :], down[1], preferred_element_type=jnp.float32))
+                                 * weight.reshape(inner * seqs, mix.shape[2])[:, :1]).astype(jnp.bfloat16)
+            to = (outer - dl) % outer
+            for ds in range(1, inner):
+                k = to * inner + ds
+                near[k] = begin(remote(eout.at[mine(there(to, ds))], back.at[k], send.at[4, k], recv.at[4, k],
+                                       there(0, ds), tp))
     far = []
-    for dl in [d for d in range(1, outer)] + [0]:
+    for dl in [d for d in range(outer - 1, -1, -1)]:
         summed = eout[mine(there(dl, 0)), :].astype(jnp.float32)
         for ds in range(1, inner):
             near[dl * inner + ds].wait_recv()
@@ -326,8 +345,8 @@
             pltpu.VMEM((seqs, width), bf16),
             pltpu.SemaphoreType.DMA((6, n)),
             pltpu.SemaphoreType.DMA((6, n)),
-            pltpu.SemaphoreType.DMA((4,)),
-            pltpu.SemaphoreType.DMA((4,)),
+            pltpu.SemaphoreType.DMA((4 + math.isqrt(n),)),
+            pltpu.SemaphoreType.DMA((4 + math.isqrt(n),)),
             pltpu.SemaphoreType.DMA((4,)),
         ],
         compiler_params=pltpu.CompilerParams(

time: 61.5 us -> 59.7 us (0.971)
  Pallas kernels: 48 us -> 46.2 us
    pallas_call x1, Pallas kernels: 48 us -> 46.2 us  [rest_kernel(): pl.pallas_call(functools.partial(rest_body, n), out_shape=jax.ShapeDtypeS...]
where the time goes in v3:
time: 59.7 us; the launch traced here: 59.5 us
  Pallas kernels  46.2 us (77%)
  matrix products  5.67 us (9%)
  local copies, waits for them, and re-layouts  4.14 us (7%)
  other arithmetic  2.54 us (4%)
  between operations  0.86 us (1%)
    pallas_call x1, Pallas kernels, rest_kernel(): pl.pallas_call(functools.partial(rest_body, n), out_shape=jax.ShapeDtypeS...  46.2 us
    dot_general x1, matrix products, attend(): jnp.dot(normed, query_weight, preferred_element_type=jnp.float32)  3.01 us
    unnamed x29, local copies, waits for them, and re-layouts  1.95 us

profile of v3, /device:TPU:1, one launch (start us, length us, event | category | flops | bytes accessed | tf_op | source)
XLA Modules:
  0.0 59.5 jit_solution(3063062689811247455)
XLA Ops:
  0.6 0.0 copy-start
  0.6 0.8 %convert_element_type.41 = f32[2048]{0:T(1024)S(1)} convert(bf16[2048]{0:T(1024)(128)(2,1)} %param.19) | non-fusion elementwise | flops 2048 | bytes 12288 | tf_op jit(solution)/shard_map/convert_element_type | solution.py:21
  1.5 1.0 %fusion.26 = f32[16]{0:T(128)S(1)} fusion(bf16[16,2048]{1,0:T(8,128)(2,1)} %hid_ref.1), kind=kLoop, calls=%fused_computation.23 | loop fusion | flops 98288 | bytes 65600 | tf_op jit(solution)/shard_map/reduce_sum | solution.py:20
  2.5 0.0 copy-start.1
  2.5 0.0 copy-start.2
  2.5 0.0 copy-start.11
  2.5 0.0 copy-start.12
  2.5 3.0 %convolution_convert_fusion = bf16[16,1024]{1,0:T(8,128)(2,1)S(1)} fusion(bf16[2048,1024]{1,0:T(8,128)(2,1)} %param.20, bf16[16,2048]{1,0:T(8,128)(2,1)} %hid_ref.1, f32[2048]{0:T(1024)S(1)} %convert_element_type.41, f32[16]{0:T(128)S(1)} %add_rsqrt_fusion), kind=kOutput, calls=%fused_computation.10 | convolution fusion | flops 67256320 | bytes 4300864 | tf_op jit(solution)/shard_map/dot_general | solution.py:33
  5.5 0.1 reshape.124
  5.7 0.1 iota_compare_fusion
  5.8 0.2 select_reduce_fusion
  5.9 0.0 copy-done.2
  6.0 0.0 copy-done.11
  6.0 0.2 fusion.30
  6.2 0.0 copy-start.5
  6.2 0.1 iota_compare_fusion.1
  6.3 0.0 copy-start.10
  6.3 0.0 copy-start.3
  6.3 0.0 copy-start.9
  6.4 0.5 fusion.39
  6.9 0.4 copy-done.10
  7.3 0.2 convolution_convert_fusion.2
  7.5 0.2 fusion.31
  7.7 0.3 fusion.23
  8.0 0.8 %fusion.40 = (f32[16,64]{1,0:T(8,128)S(1)}, bf16[16,64]{1,0:T(8,128)(2,1)}) fusion(bf16[2048,64]{0,1:T(8,128)(2,1)S(1)} %copy-done.3, bf16[16,2048]{1,0:T(8,128)(2,1)S(1)} %copy-done.2, f32[2048]{0:T(1024)S(1)} %convert_element_type.41, f32[16]{0:T(128)S(1)} %add_rsqrt_fusion), kind=kOutput, calls=%fused_computation.44 | convolution fusion | flops 4327424 | bytes 342080 | tf_op jit(solution)/shard_map/dot_general | solution.py:40
  8.9 0.7 %fusion.19 = bf16[16,16,64]{2,1,0:T(8,128)(2,1)S(1)} fusion(bf16[16,1,64,1024]{3,2,1,0:T(8,128)(2,1)S(1)} %copy-done.9, f32[16,16,1024]{2,1,0:T(8,128)S(1)} %get-tuple-element.7, f32[16,16]{1,0:T(8,128)S(1)} %get-tuple-element.5, f32[16,16]{1,0:T(8,128)S(1)} %multiply_maximum_fusion, f32[16,64]{1,0:T(8,128)S(1)} %get-tuple-element.8, ...), kind=kOutput, calls=%fused_computation.9 | convolution fusion | flops 34390016 | bytes 3185664 | tf_op jit(solution)/shard_map/sgjp,sgdp->sgjd/dot_general | solution.py:68
  9.6 0.0 copy-done.13
  9.6 0.7 %convert_element_type.51.att_ref = bf16[16,1024]{1,0:T(8,128)(2,1)} reshape(bf16[16,16,64]{2,1,0:T(8,128)(2,1)S(1)} %fusion.19) | data formatting | bytes 65536 | tf_op jit(solution)/shard_map/convert_element_type | solution.py:79
  10.4 0.7 %broadcast_in_dim.65.mix_ref = f32[16,16,128]{2,1,0:T(8,128)} broadcast(f32[16,16]{1,0:T(8,128)S(1)} %select_reduce_fusion.1), dimensions={0,1} | broadcast | bytes 132096 | tf_op jit(solution)/shard_map/broadcast_in_dim | solution.py:319
  11.1 0.6 %broadcast_in_dim.62.gain_ref = bf16[1,2048]{1,0:T(2,128)(2,1)} reshape(bf16[2048]{0:T(1024)(128)(2,1)S(1)} %copy-done.6) | data formatting | bytes 8192 | tf_op jit(solution)/shard_map/broadcast_in_dim | solution.py:354
  11.7 46.2 %shard_map.201 = bf16[16,2048]{1,0:T(8,128)(2,1)} custom-call(bf16[16,1024]{1,0:T(8,128)(2,1)} %convert_element_type.51.att_ref, bf16[16,2048]{1,0:T(8,128)(2,1)} %hid_ref.1, bf16[1,2048]{1,0:T(2,128)(2,1)} %broadcast_in_dim.62.gain_ref, f32[16,16,128]{2,1,0:T(8,128)} %broadcast_in_dim.65.mix_ref, bf16[128,2048]{1,0:T(8,128)(2,1)} %ow_hbm.1, ...), custom_call_target="tpu_custom_call" | custom-call | tf_op jit(solution)/shard_map/pallas_call | solution.py:323
  58.0 1.5 %copy.29 = bf16[16,2048]{1,0:T(8,128)(2,1)} copy(bf16[16,2048]{1,0:T(8,128)(2,1)} %shard_map.201) | data formatting | bytes 131072
  (22 shorter events, 0.1 us)
Async XLA Ops:
  0.6 5.7 %copy-start = (bf16[16,1,64,1024]{3,2,1,0:T(8,128)(2,1)S(1)}, bf16[16,1,64,1024]{3,2,1,0:T(8,128)(2,1)}, u32[]{:S(2)}) copy-start(bf16[16,1,64,1024]{3,2,1,0:T(8,128)(2,1)} %param.25) | copy-start | bytes 6291460
  2.5 3.2 %copy-start.8 = (s32[16]{0:T(128)S(1)}, s32[16]{0:T(128)}, u32[]{:S(2)}) copy-start(s32[16]{0:T(128)} %param.28) | copy-start | bytes 196
  2.5 3.3 %copy-start.1 = (f32[16,16,1024]{2,1,0:T(8,128)S(1)}, f32[16,16,1024]{2,1,0:T(8,128)}, u32[]{:S(2)}) copy-start(f32[16,16,1024]{2,1,0:T(8,128)} %param.27) | copy-start | bytes 3145732
  2.5 3.5 %copy-start.2 = (bf16[16,2048]{1,0:T(8,128)(2,1)S(1)}, bf16[16,2048]{1,0:T(8,128)(2,1)}, u32[]{:S(2)}) copy-start(bf16[16,2048]{1,0:T(8,128)(2,1)} %hid_ref.1) | copy-start | bytes 196612
  2.5 3.5 %copy-start.11 = (bf16[2048,16]{0,1:T(8,128)(2,1)S(1)}, bf16[2048,16]{0,1:T(8,128)(2,1)}, u32[]{:S(2)}) copy-start(bf16[2048,16]{0,1:T(8,128)(2,1)} %param.23) | copy-start | bytes 196612
  2.5 3.5 %copy-start.12 = (f32[16]{0:T(128)S(1)}, f32[16]{0:T(128)}, u32[]{:S(2)}) copy-start(f32[16]{0:T(128)} %param.24) | copy-start | bytes 196
  6.2 0.7 %copy-start.5 = (f32[16,16]{1,0:T(8,128)}, f32[16,16]{1,0:T(8,128)S(1)}, u32[]{:S(2)}) copy-start(f32[16,16]{1,0:T(8,128)S(1)} %fusion.30) | copy-start | bytes 3076
  6.3 1.0 %copy-start.10 = (bf16[2048,64]{0,1:T(8,128)(2,1)S(1)}, bf16[2048,64]{0,1:T(8,128)(2,1)}, u32[]{:S(2)}) copy-start(bf16[2048,64]{0,1:T(8,128)(2,1)} %param.21) | copy-start | bytes 786436
  6.3 1.7 %copy-start.3 = (bf16[2048,64]{0,1:T(8,128)(2,1)S(1)}, bf16[2048,64]{0,1:T(8,128)(2,1)}, u32[]{:S(2)}) copy-start(bf16[2048,64]{0,1:T(8,128)(2,1)} %param.22) | copy-start | bytes 786436
  6.3 2.5 %copy-start.9 = (bf16[16,1,64,1024]{3,2,1,0:T(8,128)(2,1)S(1)}, bf16[16,1,64,1024]{3,2,1,0:T(8,128)(2,1)}, u32[]{:S(2)}) copy-start(bf16[16,1,64,1024]{3,2,1,0:T(8,128)(2,1)} %param.26) | copy-start | bytes 6291460
  7.5 2.1 %copy-start.13 = (bf16[16,64]{1,0:T(8,128)(2,1)}, bf16[16,64]{1,0:T(8,128)(2,1)S(1)}, u32[]{:S(2)}) copy-start(bf16[16,64]{1,0:T(8,128)(2,1)S(1)} %convolution_convert_fusion.2) | copy-start | bytes 6148
  8.9 1.5 %copy-start.4 = (f32[16,6]{0,1:T(8,128)S(1)}, f32[16,6]{0,1:T(8,128)}, u32[]{:S(2)}) copy-start(f32[16,6]{0,1:T(8,128)} %param.32) | copy-start | bytes 1156
  8.9 1.5 %copy-start.7 = (s32[16,6]{0,1:T(8,128)S(1)}, s32[16,6]{0,1:T(8,128)}, u32[]{:S(2)}) copy-start(s32[16,6]{0,1:T(8,128)} %param.31) | copy-start | bytes 1156
  8.9 2.3 %copy-start.6 = (bf16[2048]{0:T(1024)(128)(2,1)S(1)}, bf16[2048]{0:T(1024)(128)(2,1)}, u32[]{:S(2)}) copy-start(bf16[2048]{0:T(1024)(128)(2,1)} %param.30) | copy-start | bytes 12292
